TPU v7x, 32 devices: a whole 2x2x4 slice. The times are simulated.
32 devices in a mesh: fs: 8 (over z, y), tp: 4 (over x, core).
Axes of the slice: x: 2, y: 2, z: 4, core: 2. Of those that a mesh axis runs over, the one named last changes fastest.
Arguments:
- layer_input: bfloat16 [16384, 2048], P('fs'), may hold values from -6 to 6
- input_cotangent: bfloat16 [16384, 2048], P('fs', 'tp'), may hold values from -6 to 6
- gate_cotangent: bfloat16 [16384, 2048], P('fs', 'tp'), may hold values from -6 to 6
- input_weight: float32 [2048, 2048], P('fs', 'tp'), may hold values from -0.125 to 0.125
- gate_weight: float32 [2048, 2048], P('fs', 'tp'), may hold values from -0.125 to 0.125
- input_basis: bfloat16 [2048, 256], P('fs'), may hold values from -1.81196113 to 1.81196113
- gate_basis: bfloat16 [2048, 256], P('fs'), may hold values from -1.81196113 to 1.81196113
- input_first: float32 [256, 2048], P('fs', 'tp'), may hold values from -10496 to 10496
- input_second: float32 [256, 2048], P('fs', 'tp'), may hold values from 16384 to 491520
- gate_first: float32 [256, 2048], P('fs', 'tp'), may hold values from -10496 to 10496
- gate_second: float32 [256, 2048], P('fs', 'tp'), may hold values from 16384 to 491520
Outputs:
- input_new: float32 [2048, 2048], P('fs', 'tp')
- gate_new: float32 [2048, 2048], P('fs', 'tp')
- input_step: float32 [2048, 2048], P('fs', 'tp')
- gate_step: float32 [2048, 2048], P('fs', 'tp')
- input_first_new: float32 [256, 2048], P('fs', 'tp')
- input_second_new: float32 [256, 2048], P('fs', 'tp')
- gate_first_new: float32 [256, 2048], P('fs', 'tp')
- gate_second_new: float32 [256, 2048], P('fs', 'tp')
- input_copy: bfloat16 [2048, 2048], P(None, 'tp')
- gate_copy: bfloat16 [2048, 2048], P(None, 'tp')
All inputs are finite; a program needn't handle non-finite values.
Results may differ from a plain program's by a relative error of at most 0.0055.
Values may be sent and summed in bfloat16 or wider, within the bound.
A program may use at most 64 MiB of HBM per device.

v0:
```python
import jax
import jax.numpy as jnp
from jax import lax
from jax.sharding import PartitionSpec as P

D = 2048
W = 2048


first_decay = 0.8
second_decay = 0.95
learn_rate = 0.01


def moments(small, first, second):
    first_new = first_decay * first + (1.0 - first_decay) * small
    second_new = second_decay * second + (1.0 - second_decay) * small * small
    direction = (first_new / (jnp.sqrt(second_new) + 1e-08)).astype(jnp.bfloat16)
    return (first_new, second_new, direction)


def split_product(projected, cotangent):
    upper = projected.astype(jnp.bfloat16)
    lower = (projected - upper.astype(jnp.float32)).astype(jnp.bfloat16)
    dims = (((0,), (0,)), ((), ()))
    return lax.dot_general(
        upper, cotangent, dims, preferred_element_type=jnp.float32
    ) + lax.dot_general(lower, cotangent, dims, preferred_element_type=jnp.float32)


def shards(
    layer_input,
    input_cotangent,
    gate_cotangent,
    input_weight,
    gate_weight,
    input_basis,
    gate_basis,
    input_first,
    input_second,
    gate_first,
    gate_second,
):
    pieces = (
        lax.all_gather(input_basis, "fs", axis=0, tiled=True),
        lax.all_gather(gate_basis, "fs", axis=0, tiled=True),
    )
    input_proj = jnp.dot(layer_input, pieces[0], preferred_element_type=jnp.float32)
    gate_proj = jnp.dot(layer_input, pieces[1], preferred_element_type=jnp.float32)
    input_small = split_product(input_proj, input_cotangent)
    gate_small = split_product(gate_proj, gate_cotangent)
    input_part, gate_part = (
        lax.psum_scatter(input_small, "fs", scatter_dimension=0, tiled=True),
        lax.psum_scatter(gate_small, "fs", scatter_dimension=0, tiled=True),
    )
    in_first, in_second, in_direction = moments(input_part, input_first, input_second)
    gt_first, gt_second, gt_direction = moments(gate_part, gate_first, gate_second)
    pieces = (
        lax.all_gather(in_direction, "fs", axis=0, tiled=True),
        lax.all_gather(gt_direction, "fs", axis=0, tiled=True),
    )
    input_update = jnp.dot(input_basis, pieces[0], preferred_element_type=jnp.float32)
    gate_update = jnp.dot(gate_basis, pieces[1], preferred_element_type=jnp.float32)
    input_squares, gate_squares = lax.psum(
        (jnp.sum(input_update * input_update), jnp.sum(gate_update * gate_update)), ("fs", "tp")
    )
    input_factor = jnp.minimum(1.0, 1.0 / jnp.sqrt(input_squares / (D * W) + 1e-06))
    gate_factor = jnp.minimum(1.0, 1.0 / jnp.sqrt(gate_squares / (D * W) + 1e-06))
    input_step = input_factor * input_update
    gate_step = gate_factor * gate_update
    input_new = input_weight - learn_rate * input_step
    gate_new = gate_weight - learn_rate * gate_step
    input_copy, gate_copy = (
        lax.all_gather(input_new.astype(jnp.bfloat16), "fs", axis=0, tiled=True),
        lax.all_gather(gate_new.astype(jnp.bfloat16), "fs", axis=0, tiled=True),
    )
    return (
        input_new,
        gate_new,
        input_step,
        gate_step,
        in_first,
        in_second,
        gt_first,
        gt_second,
        input_copy,
        gate_copy,
    )


def solution(mesh):
    placed = (
        P("fs", None),
        P("fs", "tp"),
        P("fs", "tp"),
        P("fs", "tp"),
        P("fs", "tp"),
        P("fs", None),
        P("fs", None),
        P("fs", "tp"),
        P("fs", "tp"),
        P("fs", "tp"),
        P("fs", "tp"),
    )
    return jax.shard_map(
        shards,
        mesh=mesh,
        in_specs=placed,
        out_specs=(
            P("fs", "tp"),
            P("fs", "tp"),
            P("fs", "tp"),
            P("fs", "tp"),
            P("fs", "tp"),
            P("fs", "tp"),
            P("fs", "tp"),
            P("fs", "tp"),
            P(None, "tp"),
            P(None, "tp"),
        ),
        check_vma=False,
    )
```

profile of v0, /device:TPU:0, one launch (start us, length us, event | category | flops | bytes accessed | tf_op | source)
XLA Modules:
  0.0 412.4 jit_solution(7743012523781812951)
XLA Ops:
  7.2 0.0 copy-start
  7.2 0.0 all-gather.7.cloned.1.call-start
  7.2 0.7 all-gather.7.cloned.1.call-update
  7.9 0.0 all-gather.5.cloned.1.call-start
  8.0 0.7 all-gather.5.cloned.1.call-update
  8.7 0.0 reduce-scatter.5.cloned.1.call-start
  8.7 44.4 %all-gather.7.cloned.1.call-done = bf16[2048,256]{1,0:T(8,128)(2,1)} async-done(((bf16[256,256]{1,0:T(8,128)(2,1)}), bf16[2048,256]{1,0:T(8,128)(2,1)}) %all-gather.7.cloned.1.call-update) | async-done | bytes 1048592 | tf_op jit(solution)/shard_map/all_gather | solution.py:46
  53.2 6.1 %fusion.13 = f32[2048,256]{1,0:T(8,128)S(1)} fusion(bf16[2048,2048]{1,0:T(8,128)(2,1)} %param.11, bf16[2048,256]{1,0:T(8,128)(2,1)} %all-gather.7.cloned.1.call-done), kind=kOutput, calls=%fused_computation.27 | convolution fusion | flops 2147483648 | bytes 11534336 | tf_op jit(solution)/shard_map/dot_general | solution.py:49
  59.3 0.8 fusion.1
  60.0 1.6 convolution_add_fusion
  61.6 0.0 reduce-scatter.5.cloned.1.call-update
  61.6 0.0 reduce-scatter.3.cloned.1.call-start
  61.7 32.6 %all-gather.5.cloned.1.call-done = bf16[2048,256]{1,0:T(8,128)(2,1)} async-done(((bf16[256,256]{1,0:T(8,128)(2,1)}), bf16[2048,256]{1,0:T(8,128)(2,1)}) %all-gather.5.cloned.1.call-update) | async-done | bytes 1048592 | tf_op jit(solution)/shard_map/all_gather | solution.py:45
  94.3 6.2 %fusion.12 = f32[2048,256]{1,0:T(8,128)S(1)} fusion(bf16[2048,2048]{1,0:T(8,128)(2,1)} %param.11, bf16[2048,256]{1,0:T(8,128)(2,1)} %all-gather.5.cloned.1.call-done), kind=kOutput, calls=%fused_computation.26 | convolution fusion | flops 2147483648 | bytes 11534336 | tf_op jit(solution)/shard_map/dot_general | solution.py:48
  100.6 0.0 copy-done.1
  100.6 0.7 fusion.4
  101.3 0.0 copy-start.5
  101.3 0.0 copy-start.6
  101.4 0.0 copy-start.7
  101.4 1.5 convolution_add_fusion.1
  102.9 0.0 reduce-scatter.3.cloned.1.call-update
  102.9 0.0 all-gather.9.cloned.1.call-start
  103.0 1.0 copy.21
  104.0 55.7 %reduce-scatter.5.cloned.1.call-done = f32[32,512]{1,0:T(8,128)} async-done(((f32[256,512]{1,0:T(8,128)}), f32[32,512]{1,0:T(8,128)}) %reduce-scatter.5.cloned.1.call-update) | async-done | bytes 65552 | tf_op jit(solution)/shard_map/reduce_scatter | solution.py:54
  159.7 0.0 copy-done.6
  159.7 1.5 divide_convert_fusion
  161.3 30.9 %all_gather.21 = bf16[256,512]{1,0:T(8,128)(2,1)S(1)} all-gather(bf16[32,512]{1,0:T(8,128)(2,1)S(1)} %get-tuple-element.28), channel_id=1, replica_groups=mesh['fs'=8,'tp'=4] {'fs'}, dimensions={0}, use_global_device_ids=true | all-gather | bytes 294912 | tf_op jit(solution)/shard_map/all_gather | solution.py:60
  192.2 0.9 multiply_reduce_fusion
  193.1 32.0 %reduce-scatter.3.cloned.1.call-done = f32[32,512]{1,0:T(8,128)} async-done(((f32[256,512]{1,0:T(8,128)}), f32[32,512]{1,0:T(8,128)}) %reduce-scatter.3.cloned.1.call-update) | async-done | bytes 65552 | tf_op jit(solution)/shard_map/reduce_scatter | solution.py:53
  225.2 0.0 copy-done.9
  225.2 1.5 divide_convert_fusion.1
  226.7 30.8 %all_gather.19 = bf16[256,512]{1,0:T(8,128)(2,1)S(1)} all-gather(bf16[32,512]{1,0:T(8,128)(2,1)S(1)} %get-tuple-element.31), channel_id=1, replica_groups=mesh['fs'=8,'tp'=4] {'fs'}, dimensions={0}, use_global_device_ids=true | all-gather | bytes 294912 | tf_op jit(solution)/shard_map/all_gather | solution.py:59
  257.5 1.7 multiply_reduce_fusion.1
  259.2 37.8 %all-reduce = (f32[]{:T(128)}, f32[]{:T(128)}) all-reduce(f32[]{:T(128)} %get-tuple-element.34, f32[]{:T(128)} %get-tuple-element.36), channel_id=1, replica_groups=mesh['fs'=8,'tp'=4] {'fs','tp'}, use_global_device_ids=true, to_apply=%region_2.0 | all-reduce | flops 2 | bytes 16 | tf_op jit(solution)/shard_map/psum | solution.py:64
  297.7 2.2 fusion.9
  299.8 0.0 all-gather.9.cloned.1.call-update
  299.9 0.0 all-gather.11.cloned.1.call-start
  299.9 2.0 copy.22
  302.6 2.2 fusion.8
  304.9 0.0 all-gather.11.cloned.1.call-update
  304.9 2.1 copy.24
  307.0 2.1 copy.26
  309.0 1.0 copy.23
  310.0 1.0 copy.25
  311.0 40.2 %all-gather.9.cloned.1.call-done = bf16[2048,512]{0,1:T(8,128)(2,1)} async-done(((bf16[256,512]{0,1:T(8,128)(2,1)}), bf16[2048,512]{0,1:T(8,128)(2,1)}) %all-gather.9.cloned.1.call-update) | async-done | bytes 2097168 | tf_op jit(solution)/shard_map/all_gather | solution.py:74
  351.2 3.9 copy.27
  355.1 46.5 %all-gather.11.cloned.1.call-done = bf16[2048,512]{0,1:T(8,128)(2,1)} async-done(((bf16[256,512]{0,1:T(8,128)(2,1)}), bf16[2048,512]{0,1:T(8,128)(2,1)}) %all-gather.11.cloned.1.call-update) | async-done | bytes 2097168 | tf_op jit(solution)/shard_map/all_gather | solution.py:75
  401.7 3.9 copy.28
  (13 shorter events, 0.0 us)
Async XLA Ops:
  7.2 52.1 %copy-start = (bf16[2048,512]{1,0:T(8,128)(2,1)S(1)}, bf16[2048,512]{1,0:T(8,128)(2,1)}, u32[]{:S(2)}) copy-start(bf16[2048,512]{1,0:T(8,128)(2,1)} %param.13) | copy-start | bytes 6291460
  7.2 46.0 %all-gather.7.cloned.1.call-start = ((), (), s32[]{:S(2)}) async-start(), calls=%async_computation.4 | async-start | bytes 1179648 | tf_op jit(solution)/shard_map/all_gather | solution.py:46
  7.9 86.4 %all-gather.5.cloned.1.call-start = ((), (), s32[]{:S(2)}) async-start(), calls=%async_computation.2 | async-start | bytes 1179648 | tf_op jit(solution)/shard_map/all_gather | solution.py:45
  8.7 151.1 %reduce-scatter.5.cloned.1.call-start = ((), (), s32[]{:S(2)}) async-start(), calls=%async_computation.5 | async-start | bytes 589824 | tf_op jit(solution)/shard_map/reduce_scatter | solution.py:54
  61.6 163.5 %reduce-scatter.3.cloned.1.call-start = ((), (), s32[]{:S(2)}) async-start(), calls=%async_computation.3 | async-start | bytes 589824 | tf_op jit(solution)/shard_map/reduce_scatter | solution.py:53
  94.3 6.2 %copy-start.1 = (bf16[2048,512]{1,0:T(8,128)(2,1)S(1)}, bf16[2048,512]{1,0:T(8,128)(2,1)}, u32[]{:S(2)}) copy-start(bf16[2048,512]{1,0:T(8,128)(2,1)} %param.12) | copy-start | bytes 6291460
  101.3 1.7 copy-start.5
  101.3 58.4 %copy-start.6 = (f32[32,512]{1,0:T(8,128)S(1)}, f32[32,512]{1,0:T(8,128)}, u32[]{:S(2)}) copy-start(f32[32,512]{1,0:T(8,128)} %param.21) | copy-start | bytes 196612
  101.4 58.4 %copy-start.7 = (f32[32,512]{1,0:T(8,128)S(1)}, f32[32,512]{1,0:T(8,128)}, u32[]{:S(2)}) copy-start(f32[32,512]{1,0:T(8,128)} %param.20) | copy-start | bytes 196612
  102.9 89.3 %copy-start.3 = (bf16[256,256]{1,0:T(8,128)(2,1)S(1)}, bf16[256,256]{1,0:T(8,128)(2,1)}, u32[]{:S(2)}) copy-start(bf16[256,256]{1,0:T(8,128)(2,1)} %param.17) | copy-start | bytes 393220
  102.9 122.3 %copy-start.8 = (f32[32,512]{1,0:T(8,128)S(1)}, f32[32,512]{1,0:T(8,128)}, u32[]{:S(2)}) copy-start(f32[32,512]{1,0:T(8,128)} %param.19) | copy-start | bytes 196612
  102.9 122.3 %copy-start.9 = (f32[32,512]{1,0:T(8,128)S(1)}, f32[32,512]{1,0:T(8,128)}, u32[]{:S(2)}) copy-start(f32[32,512]{1,0:T(8,128)} %param.18) | copy-start | bytes 196612
  102.9 154.6 %copy-start.4 = (bf16[256,256]{1,0:T(8,128)(2,1)S(1)}, bf16[256,256]{1,0:T(8,128)(2,1)}, u32[]{:S(2)}) copy-start(bf16[256,256]{1,0:T(8,128)(2,1)} %param.16) | copy-start | bytes 393220
  102.9 248.3 %all-gather.9.cloned.1.call-start = ((), (), s32[]{:S(2)}) async-start(), calls=%async_computation.6 | async-start | bytes 2359296 | tf_op jit(solution)/shard_map/all_gather | solution.py:74
  299.9 101.8 %all-gather.11.cloned.1.call-start = ((), (), s32[]{:S(2)}) async-start(), calls=%async_computation.7 | async-start | bytes 2359296 | tf_op jit(solution)/shard_map/all_gather | solution.py:75
  304.9 4.2 %copy-start.2 = (f32[256,512]{0,1:T(8,128)S(1)}, f32[256,512]{0,1:T(8,128)}, u32[]{:S(2)}) copy-start(f32[256,512]{0,1:T(8,128)} %get-tuple-element.26) | copy-start | bytes 1572868
Sparse Core Ops, SparseCore 0:
  10.1 42.9 all-gather.6
  55.3 39.0 all-gather.4
  98.3 61.4 reduce-scatter.4
  163.5 61.6 reduce-scatter.2
  300.0 51.1 all-gather.8
  353.1 48.5 all-gather.10
where the time goes:
time: 413 us; the launch traced here: 412 us
  waiting for transfers between devices  253 us (61%)
  blocking collectives  99.5 us (24%)
  matrix products  19.5 us (5%)
  local copies, waits for them, and re-layouts  17.1 us (4%)
  between operations  15.6 us (4%)
  other arithmetic  7.44 us (2%)
    reduce_scatter x1, waiting for transfers between devices, shards(): lax.psum_scatter(gate_small, 'fs', scatter_dimension=0, tiled=True)  55.7 us
    all_gather x1, waiting for transfers between devices, shards(): lax.all_gather(gate_new.astype(jnp.bfloat16), 'fs', axis=0, tiled=True)  46.5 us
    all_gather x1, waiting for transfers between devices, shards(): lax.all_gather(gate_basis, 'fs', axis=0, tiled=True)  44.4 us
    all_gather x1, waiting for transfers between devices, shards(): lax.all_gather(input_new.astype(jnp.bfloat16), 'fs', axis=0, tiled=True)  40.2 us
    psum x1, blocking collectives, shards(): lax.psum((jnp.sum(input_update * input_update), jnp.sum(gate_update * gat...  37.8 us
    all_gather x1, waiting for transfers between devices, shards(): lax.all_gather(input_basis, 'fs', axis=0, tiled=True)  32.6 us
    reduce_scatter x1, waiting for transfers between devices, shards(): lax.psum_scatter(input_small, 'fs', scatter_dimension=0, tiled=True)  32 us
    all_gather x1, blocking collectives, shards(): lax.all_gather(gt_direction, 'fs', axis=0, tiled=True)  30.9 us
  transfers between devices with their start and end apart: 6, of which 6 were waited for; matrix products, arithmetic and copies ran while one was open for 8% of the time, Pallas kernels for 0%

commit v1 on v0

v1 whole, which is shorter than its diff:
```python
import functools

import jax
import jax.numpy as jnp
from jax import lax
from jax.experimental import pallas as pl
from jax.experimental.pallas import tpu as pltpu
from jax.sharding import PartitionSpec as P

first_decay = 0.8
second_decay = 0.95
learn_rate = 0.01
ANY = pl.BlockSpec(memory_space=pl.ANY)
VMEM = pl.BlockSpec(memory_space=pltpu.VMEM)
MESH = pl.DeviceIdType.MESH
f32, bf16 = jnp.float32, jnp.bfloat16


def moments(small, first, second):
    first_new = first_decay * first + (1.0 - first_decay) * small
    second_new = second_decay * second + (1.0 - second_decay) * small * small
    return first_new, second_new


def remote(src, dst, send, recv, **axis):
    return pltpu.make_async_remote_copy(
        src_ref=src, dst_ref=dst, send_sem=send, recv_sem=recv, device_id=axis, device_id_type=MESH
    )


def exchange(
    n, tp, x_hbm, ci_hbm, cg_hbm, wi_hbm, wg_hbm, bi_hbm, bg_hbm, first, second,
    weights, basis_out, dir_out, small_out, squares_out,
    xs, cs, ball, wf, wb, proj, acc, part, recvp, dirs, dirf, sq,
    xsem, csem, bsem, wsem, osem,
    b_s, b_r, x_s, x_r, c_s, c_r, d_s, d_r, p_s, p_r, g_s, g_r, q_s, q_r,
    r_s, r_r, l_s, l_r, y_s, y_r,
):
    me, t = lax.axis_index("fs"), lax.axis_index("tp")
    tokens, rb, rank2 = xs.shape[1], ball.shape[1], ball.shape[2]
    group = xs.shape[2] // rb
    rank = rank2 // 2
    rr = rank // n
    wc = cs.shape[2]
    quarter = rb // 4
    tile = min(512, tokens)

    def local(src, dst, sem):
        copy = pltpu.make_async_copy(src, dst, sem)
        copy.start()
        return copy

    def peer(k):
        return lax.rem(me + k, n)

    def origin(k):
        return lax.rem(me + n - k, n)

    b_in = [
        local(ref, ball.at[me, :, pl.ds(p * rank, rank)], bsem.at[p])
        for p, ref in enumerate((bi_hbm, bg_hbm))
    ]
    x_in = []
    wide = rb * group
    for k in range(n // group):
        at = pl.multiple_of(origin(k) * rb, rb) if group == 1 else k * wide
        x_in.append(local(x_hbm.at[:, pl.ds(at, wide)], xs.at[k], xsem.at[k]))
    w_in = [local(ref, wf.at[p], wsem.at[p]) for p, ref in enumerate((wi_hbm, wg_hbm))]
    c_in = [local(ref, cs.at[p], csem.at[p]) for p, ref in enumerate((ci_hbm, cg_hbm))]

    barrier = pltpu.get_barrier_semaphore()
    for k in range(1, n):
        pl.semaphore_signal(barrier, inc=1, device_id={"fs": peer(k)}, device_id_type=MESH)
    for k in range(1, tp):
        pl.semaphore_signal(barrier, inc=1, device_id={"tp": lax.rem(t + k, tp)}, device_id_type=MESH)
    pl.semaphore_wait(barrier, n + tp - 2)

    q = lax.rem(t, 4)
    base = t - q
    qx = lax.rem(q + 2, 4)
    qc = q + 1 - 2 * lax.rem(q, 2)
    qd = lax.rem(qc + 2, 4)

    def rows(j, which):
        return ball.at[j, pl.ds(pl.multiple_of(which * quarter, quarter), quarter), :]

    for copy in b_in:
        copy.wait()
    pending = []
    b_copies = {}
    for k in range(1, n):
        b_copies[k] = remote(rows(me, q), rows(me, q), b_s.at[k], b_r.at[k], fs=peer(k))
        b_copies[k].start()
        pending.append(b_copies[k])

    def product(k, j):
        x_in[k].wait()

        def body(i, _):
            at = pl.ds(pl.multiple_of(i * tile, tile), tile)
            right = ball[j] if group == 1 else ball[j:j + group].reshape(wide, rank2)
            term = jnp.dot(xs[k, at, :], right, preferred_element_type=f32)
            if k == 0:
                proj[at, :] = term
            else:
                proj[at, :] += term
            return 0

        lax.fori_loop(0, tokens // tile, body, 0)

    def got(ref, sem):
        pltpu.make_async_copy(ref, ref, sem).wait()

    for k in range(n + 2):
        if 1 <= k < n:
            j = origin(k)
            got(rows(j, q), b_r.at[k])
            for ss, sr, to in ((x_s, x_r, qx), (c_s, c_r, qc)):
                copy = remote(rows(j, q), rows(j, q), ss.at[k], sr.at[k], tp=base + to)
                copy.start()
                pending.append(copy)
        if 1 <= k - 1 < n:
            j = origin(k - 1)
            got(rows(j, qx), x_r.at[k - 1])
            copy = remote(rows(j, qx), rows(j, qx), d_s.at[k - 1], d_r.at[k - 1], tp=base + qc)
            copy.start()
            pending.append(copy)
        if k == 0:
            if group == 1:
                product(0, me)
            for p in range(2):
                w_in[p].wait()
                wb[p] = wf[p].astype(bf16)
        if k >= 3:
            j = origin(k - 2)
            got(rows(j, qc), c_r.at[k - 2])
            got(rows(j, qd), d_r.at[k - 2])
            if group == 1:
                product(k - 2, j)
    if group > 1:
        for k in range(n // group):
            product(k, k * group)

    length = n // 2
    a, b = me // 2, lax.rem(me, 2)
    waits = []

    def guarded(here, copy, start=True):
        if start:
            @pl.when(here)
            def _():
                copy.start()
        waits.append((here, copy))

    def block(chain, side):
        safe = jnp.clip(chain, 0, length - 1)
        return weights.at[safe * 2 + side]

    def send_weights(s):
        for sign, ss, sr in ((1, r_s, r_r), (-1, l_s, l_r)):
            chain = a - sign * (s - 1)
            exists = jnp.logical_and(chain >= 0, chain < length)
            place = block(chain, b)
            src = wb if s == 1 else place
            slot = (s - 1) * 2 + (0 if sign == 1 else 1)
            if s > 1:
                @pl.when(exists)
                def _():
                    got(place, sr.at[s - 1])
            if s < length:
                after = a + sign
                inside = jnp.logical_and(after >= 0, after < length)
                to = jnp.clip(after, 0, length - 1) * 2 + b
                guarded(jnp.logical_and(exists, inside), remote(src, place, ss.at[s], sr.at[s], fs=to))
            if s > 1 or sign == 1:
                guarded(exists, remote(src, place, y_s.at[slot], y_r.at[slot], fs=a * 2 + 1 - b))

    send_weights(1)

    for p in range(2):
        c_in[p].wait()

        def body(i, _):
            at = pl.ds(pl.multiple_of(i * tile, tile), tile)
            term = lax.dot_general(
                proj[at, p * rank:(p + 1) * rank].astype(bf16), cs[p, at, :],
                (((0,), (0,)), ((), ())), preferred_element_type=f32,
            )
            acc[p] += term
            return 0

        acc[p] = jnp.zeros_like(acc[p])
        lax.fori_loop(0, tokens // tile, body, 0)
        for j in range(n):
            part[j, p] = acc[p, j * rr:(j + 1) * rr, :].astype(bf16)
    for k in range(1, n):
        copy = remote(part.at[peer(k)], recvp.at[k], p_s.at[k], p_r.at[k], fs=peer(k))
        copy.start()
        pending.append(copy)
    out_basis = local(ball, basis_out, osem.at[0])
    send_weights(2)
    own = pl.ds(pl.multiple_of(me * rr, rr), rr)
    total = acc[:, own, :]
    for k in range(1, n):
        got(recvp.at[k], p_r.at[k])
        total = total + recvp[k].astype(f32)
    small_out[...] = total
    first_new, second_new = moments(total, first[...], second[...])
    dirs[0] = (first_new / (jnp.sqrt(second_new) + 1e-08)).astype(bf16)
    for k in range(1, n):
        copy = remote(dirs.at[0], dirs.at[k], g_s.at[k], g_r.at[k], fs=peer(k))
        copy.start()
        pending.append(copy)
    for s in range(3, length + 1):
        if s == 3:
            send_weights(s)
    dirf[:, own, :] = dirs[0].astype(f32)
    for k in range(1, n):
        got(dirs.at[k], g_r.at[k])
        dirf[:, pl.ds(pl.multiple_of(origin(k) * rr, rr), rr), :] = dirs[k].astype(f32)
    for p in range(2):
        dir_out[p] = dirf[p].astype(bf16)
        sq[0, p] = jnp.zeros_like(sq[0, p])

        def body(j, _):
            update = jnp.dot(
                ball[j, :, p * rank:(p + 1) * rank], dir_out[p], preferred_element_type=f32
            )
            square = jnp.sum((update * update).reshape(rb // 8, 8, wc), axis=0)
            lanes = square[:, :128]
            for at in range(128, wc, 128):
                lanes = lanes + square[:, at:at + 128]
            sq[0, p] += lanes
            return 0

        lax.fori_loop(0, n, body, 0)
    for k in range(1, tp):
        copy = remote(sq.at[0], sq.at[k], q_s.at[k], q_r.at[k], tp=lax.rem(t + k, tp))
        copy.start()
        pending.append(copy)
    for s in range(4, length + 1):
        send_weights(s)
    summed = sq[0]
    for k in range(1, tp):
        got(sq.at[k], q_r.at[k])
        summed = summed + sq[k]
    squares_out[...] = summed
    out_basis.wait()
    for s in range(1, length + 1):
        for sign in (1, -1):
            if s == 1 and sign == -1:
                continue
            chain = a - sign * (s - 1)
            slot = (s - 1) * 2 + (0 if sign == 1 else 1)

            @pl.when(jnp.logical_and(chain >= 0, chain < length))
            def _():
                got(block(chain, 1 - b), y_r.at[slot])
    for here, copy in waits:
        @pl.when(here)
        def _():
            copy.wait_send()
    for copy in pending:
        copy.wait_send()


def finish(
    wi, wg, all_w, ball, dirs, small, squares, first, second, count_ref,
    new_i, new_g, step_i, step_g, fi, si, fg, sg, copy_i, copy_g,
):
    j = pl.program_id(0)
    me = lax.axis_index("fs")
    rank = dirs.shape[1]

    @pl.when(j == 0)
    def _():
        first_new, second_new = moments(small[...], first[...], second[...])
        fi[...], fg[...] = first_new[0], first_new[1]
        si[...], sg[...] = second_new[0], second_new[1]

    for p, (w, new, step, copy) in enumerate(((wi, new_i, step_i, copy_i), (wg, new_g, step_g, copy_g))):
        mean = jnp.sum(squares[p], keepdims=True) * count_ref[0]
        factor = jnp.minimum(1.0, 1.0 / jnp.sqrt(mean + 1e-06))
        update = jnp.dot(ball[0, :, p * rank:(p + 1) * rank], dirs[p], preferred_element_type=f32)
        scaled = factor * update

        @pl.when(j == me)
        def _():
            step[...] = scaled
            fresh = w[...] - learn_rate * scaled
            new[...] = fresh
            copy[...] = fresh.astype(bf16)

        @pl.when(j != me)
        def _():
            copy[...] = (all_w[0, p].astype(f32) - learn_rate * scaled).astype(bf16)


def shards(n, tp, x, ci, cg, wi, wg, bi, bg, fi, si, fg, sg):
    tokens, width = x.shape
    wc, (rb, rank), rr = ci.shape[1], bi.shape, fi.shape[0]
    length = n // 2
    group = max(1, 128 // rb)
    first, second = jnp.stack([fi, fg]), jnp.stack([si, sg])
    dma = pltpu.SemaphoreType.DMA
    all_w, ball, dirs, small, squares = pl.pallas_call(
        functools.partial(exchange, n, tp),
        out_shape=(
            jax.ShapeDtypeStruct((n, 2, rb, wc), bf16),
            jax.ShapeDtypeStruct((n, rb, 2 * rank), bf16),
            jax.ShapeDtypeStruct((2, rank, wc), bf16),
            jax.ShapeDtypeStruct((2, rr, wc), f32),
            jax.ShapeDtypeStruct((2, 8, 128), f32),
        ),
        in_specs=[ANY] * 7 + [VMEM] * 2,
        out_specs=(ANY, ANY, VMEM, VMEM, VMEM),
        scratch_shapes=[
            pltpu.VMEM((n // group, tokens, rb * group), bf16),
            pltpu.VMEM((2, tokens, wc), bf16),
            pltpu.VMEM((n, rb, 2 * rank), bf16),
            pltpu.VMEM((2, rb, wc), f32),
            pltpu.VMEM((2, rb, wc), bf16),
            pltpu.VMEM((tokens, 2 * rank), f32),
            pltpu.VMEM((2, rank, wc), f32),
            pltpu.VMEM((n, 2, rr, wc), bf16),
            pltpu.VMEM((n, 2, rr, wc), bf16),
            pltpu.VMEM((n, 2, rr, wc), bf16),
            pltpu.VMEM((2, rank, wc), f32),
            pltpu.VMEM((tp, 2, 8, 128), f32),
            dma((n,)), dma((2,)), dma((2,)), dma((2,)), dma((1,)),
        ]
        + [dma((n,))] * 12
        + [dma((tp,))] * 2
        + [dma((length + 1,))] * 4
        + [dma((2 * length,))] * 2,
        compiler_params=pltpu.CompilerParams(
            collective_id=0, has_side_effects=True, vmem_limit_bytes=56 * 1024 * 1024
        ),
        name="exchange",
    )(x, ci, cg, wi, wg, bi, bg, first, second)

    def whole(*shape):
        return pl.BlockSpec(shape, lambda j: (0,) * len(shape))

    count = jnp.full((1,), 1.0 / (width * wc * tp), f32)
    return pl.pallas_call(
        finish,
        grid=(n,),
        out_shape=tuple(jax.ShapeDtypeStruct((rb, wc), f32) for _ in range(4))
        + tuple(jax.ShapeDtypeStruct((rr, wc), f32) for _ in range(4))
        + tuple(jax.ShapeDtypeStruct((width, wc), bf16) for _ in range(2)),
        in_specs=[
            whole(rb, wc), whole(rb, wc),
            pl.BlockSpec((1, 2, rb, wc), lambda j: (j, 0, 0, 0)),
            pl.BlockSpec((1, rb, 2 * rank), lambda j: (j, 0, 0)),
            whole(2, rank, wc), whole(2, rr, wc), whole(2, 8, 128), whole(2, rr, wc), whole(2, rr, wc),
            pl.BlockSpec(memory_space=pltpu.SMEM),
        ],
        out_specs=tuple(whole(rb, wc) for _ in range(4))
        + tuple(whole(rr, wc) for _ in range(4))
        + tuple(pl.BlockSpec((rb, wc), lambda j: (j, 0)) for _ in range(2)),
        compiler_params=pltpu.CompilerParams(vmem_limit_bytes=40 * 1024 * 1024),
        name="finish",
    )(wi, wg, all_w, ball, dirs, small, squares, first, second, count)


def solution(mesh):
    cut, rows = P("fs", "tp"), P("fs", None)
    return jax.shard_map(
        functools.partial(shards, mesh.shape["fs"], mesh.shape["tp"]),
        mesh=mesh,
        in_specs=(rows, cut, cut, cut, cut, rows, rows, cut, cut, cut, cut),
        out_specs=(cut,) * 8 + (P(None, "tp"),) * 2,
        check_vma=False,
    )
```

time: 413 us -> 123 us (0.30)
  waiting for transfers between devices: 253 us -> 0 us
  Pallas kernels: 0 us -> 114 us
  blocking collectives: 99.5 us -> 0 us
  matrix products: 19.5 us -> 0 us
  between operations: 15.6 us -> 0.71 us
  local copies, waits for them, and re-layouts: 17.1 us -> 6.43 us
  other arithmetic: 7.44 us -> 1.65 us
    all_gather x4 -> x0, waiting for transfers between devices: 164 us -> none  [the longest x1 46.5 us: shards(): lax.all_gather(gate_new.astype(jnp.bfloat16), 'fs', axis=0, tiled=True)]
    pallas_call x0 -> x2, Pallas kernels: none -> 114 us  [the longest x1 107 us: shards(): pl.pallas_call(functools.partial(exchange, n, tp), out_shape=(jax.ShapeDt...]
    reduce_scatter x2 -> x0, waiting for transfers between devices: 87.8 us -> none  [the longest x1 55.7 us: shards(): lax.psum_scatter(gate_small, 'fs', scatter_dimension=0, tiled=True)]
    all_gather x2 -> x0, blocking collectives: 61.8 us -> none  [the longest x1 30.9 us: shards(): lax.all_gather(gt_direction, 'fs', axis=0, tiled=True)]
    psum x1 -> x0, blocking collectives: 37.8 us -> none  [shards(): lax.psum((jnp.sum(input_update * input_update), jnp.sum(gate_update * gat...]
    dot_general x8 -> x0, matrix products: 19.5 us -> none  [the longest x1 6.24 us: shards(): jnp.dot(layer_input, pieces[0], preferred_element_type=jnp.float32)]
    unnamed x28 -> x18, local copies, waits for them, and re-layouts: 17.1 us -> 6.43 us
    convert_element_type x4 -> x0, other arithmetic: 7.44 us -> none  [the longest x2 3.04 us: moments(): (first_new / (jnp.sqrt(second_new) + 1e-08)).astype(jnp.bfloat16)]
  transfers between devices with their start and end apart: 6 -> 0, of which waited for: 6 -> 0; matrix products, arithmetic and copies ran while one was open for 8% -> 0% of each run, Pallas kernels for 0% -> 0%
where the time goes in v1:
time: 123 us; the launch traced here: 122 us
  Pallas kernels  114 us (93%)
  local copies, waits for them, and re-layouts  6.43 us (5%)
  other arithmetic  1.65 us (1%)
    pallas_call x1, Pallas kernels, shards(): pl.pallas_call(functools.partial(exchange, n, tp), out_shape=(jax.ShapeDt...  107 us
    pallas_call x1, Pallas kernels, shards(): pl.pallas_call(finish, grid=(n,), out_shape=tuple((jax.ShapeDtypeStruct((...  7.03 us
    unnamed x18, local copies, waits for them, and re-layouts  6.43 us

profile of v1, /device:TPU:0, one launch (start us, length us, event | category | flops | bytes accessed | tf_op | source)
XLA Modules:
  0.0 122.4 jit_solution(14009476807847800670)
XLA Ops:
  0.6 1.7 %pad_maximum_fusion = (f32[2,32,512]{2,1,0:T(8,128)}, f32[2,32,512]{2,1,0:T(8,128)}) fusion(f32[1,32,512]{2,1,0:T(8,128)} %bitcast.4, f32[1,32,512]{2,1,0:T(8,128)} %bitcast.5, f32[1,32,512]{2,1,0:T(8,128)} %bitcast.6, f32[1,32,512]{2,1,0:T(8,128)} %bitcast.7), kind=kLoop, calls=%fused_computation | loop fusion | flops 65536 | bytes 524288 | tf_op jit(solution)/shard_map/stack | solution.py:304
  2.3 0.0 copy-start.1
  2.3 0.0 copy-start.2
  2.3 0.0 copy-start.4
  2.3 0.0 copy-start.5
  2.3 106.5 %exchange.1 = (bf16[8,2,256,512]{3,2,1,0:T(8,128)(2,1)}, bf16[8,256,512]{2,1,0:T(8,128)(2,1)}, bf16[2,256,512]{2,1,0:T(8,128)(2,1)}, f32[2,32,512]{2,1,0:T(8,128)}, f32[2,8,128]{2,1,0:T(8,128)}) custom-call(bf16[2048,2048]{1,0:T(8,128)(2,1)} %x_hbm.1, bf16[2048,512]{1,0:T(8,128)(2,1)} %ci_hbm.1, bf16[2048,512]{1,0:T(8,128)(2,1)} %cg_hbm.1, f32[256,512]{1,0:T(8,128)} %wi.1, ...), custom_call_target="tpu_custom_call" | custom-call | tf_op jit(solution)/shard_map/exchange/pallas_call | solution.py:306
  108.9 0.0 copy-done.1
  108.9 0.0 copy-done.2
  108.9 0.0 copy-done.4
  108.9 0.0 copy-done.5
  108.9 0.0 copy-start
  108.9 2.2 %copy-done = bf16[8,2,256,512]{3,2,1,0:T(8,128)(2,1)S(1)} copy-done((bf16[8,2,256,512]{3,2,1,0:T(8,128)(2,1)S(1)}, bf16[8,2,256,512]{3,2,1,0:T(8,128)(2,1)}, u32[]{:S(2)}) %copy-start) | copy-done | bytes 4194328
  111.1 0.0 copy-start.3
  111.1 1.6 %copy-done.3 = bf16[8,256,512]{2,1,0:T(8,128)(2,1)S(1)} copy-done((bf16[8,256,512]{2,1,0:T(8,128)(2,1)S(1)}, bf16[8,256,512]{2,1,0:T(8,128)(2,1)}, u32[]{:S(2)}) %copy-start.3) | copy-done | bytes 2097176
  112.7 0.0 copy-start.6
  112.7 1.0 copy-done.6
  113.7 0.0 copy-start.7
  113.7 0.9 copy-done.7
  114.6 0.0 copy-start.8
  114.6 0.7 copy-done.8
  115.3 7.0 %finish.1 = (f32[256,512]{1,0:T(8,128)}, f32[256,512]{1,0:T(8,128)}, f32[256,512]{1,0:T(8,128)}, f32[256,512]{1,0:T(8,128)}, f32[32,512]{1,0:T(8,128)}, /*index=...) custom-call(f32[256,512]{1,0:T(8,128)S(1)} %copy-done.1, ...), custom_call_target="tpu_custom_call" | custom-call | tf_op jit(solution)/shard_map/finish/pallas_call | solution.py:346
Async XLA Ops:
  2.3 106.6 %copy-start.1 = (f32[256,512]{1,0:T(8,128)S(1)}, f32[256,512]{1,0:T(8,128)}, u32[]{:S(2)}) copy-start(f32[256,512]{1,0:T(8,128)} %wi.1) | copy-start | bytes 1572868
  2.3 106.6 %copy-start.2 = (f32[256,512]{1,0:T(8,128)S(1)}, f32[256,512]{1,0:T(8,128)}, u32[]{:S(2)}) copy-start(f32[256,512]{1,0:T(8,128)} %wg.1) | copy-start | bytes 1572868
  2.3 106.6 %copy-start.4 = (f32[2,32,512]{2,1,0:T(8,128)S(1)}, f32[2,32,512]{2,1,0:T(8,128)}, u32[]{:S(2)}) copy-start(f32[2,32,512]{2,1,0:T(8,128)} %get-tuple-element.20.first) | copy-start | bytes 393220
  2.3 106.6 %copy-start.5 = (f32[2,32,512]{2,1,0:T(8,128)S(1)}, f32[2,32,512]{2,1,0:T(8,128)}, u32[]{:S(2)}) copy-start(f32[2,32,512]{2,1,0:T(8,128)} %get-tuple-element.21.second) | copy-start | bytes 393220
  108.9 2.2 %copy-start = (bf16[8,2,256,512]{3,2,1,0:T(8,128)(2,1)S(1)}, bf16[8,2,256,512]{3,2,1,0:T(8,128)(2,1)}, u32[]{:S(2)}) copy-start(bf16[8,2,256,512]{3,2,1,0:T(8,128)(2,1)} %get-tuple-element.15.all_w) | copy-start | bytes 12582916
  111.1 1.6 %copy-start.3 = (bf16[8,256,512]{2,1,0:T(8,128)(2,1)S(1)}, bf16[8,256,512]{2,1,0:T(8,128)(2,1)}, u32[]{:S(2)}) copy-start(bf16[8,256,512]{2,1,0:T(8,128)(2,1)} %get-tuple-element.16.ball) | copy-start | bytes 6291460
  112.7 1.0 copy-start.6
  113.7 0.9 copy-start.7
  114.6 0.7 copy-start.8

commit v2 on v1

--- a/solution.py
+++ b/solution.py
@@ -29,7 +29,7 @@
 
 
 def exchange(
-    n, tp, x_hbm, ci_hbm, cg_hbm, wi_hbm, wg_hbm, bi_hbm, bg_hbm, first, second,
+    n, tp, x_hbm, ci_hbm, cg_hbm, wi_hbm, wg_hbm, bi_hbm, bg_hbm, fi, si, fg, sg,
     weights, basis_out, dir_out, small_out, squares_out,
     xs, cs, ball, wf, wb, proj, acc, part, recvp, dirs, dirf, sq,
     xsem, csem, bsem, wsem, osem,
@@ -110,6 +110,55 @@
 
     def got(ref, sem):
         pltpu.make_async_copy(ref, ref, sem).wait()
+
+    length = n // 2
+    a, b = me // 2, lax.rem(me, 2)
+    waits = []
+
+    def block(chain, side, p):
+        return weights.at[jnp.clip(chain, 0, length - 1) * 2 + side, p]
+
+    def guarded(here, copy):
+        @pl.when(here)
+        def _():
+            copy.start()
+
+        waits.append((here, copy))
+
+    def across(s, sign, p):
+        chain = a - sign * (s - 1)
+        exists = jnp.logical_and(chain >= 0, chain < length)
+        place = block(chain, b, p)
+        slot = ((s - 1) * 2 + (0 if sign == 1 else 1)) * 2 + p
+        guarded(exists, remote(
+            wb.at[p] if s == 1 else place, place, y_s.at[slot], y_r.at[slot], fs=a * 2 + 1 - b))
+
+    def along(s, sign, p):
+        chain = a - sign * (s - 1)
+        exists = jnp.logical_and(chain >= 0, chain < length)
+        place = block(chain, b, p)
+        ss, sr = (r_s, r_r) if sign == 1 else (l_s, l_r)
+        if s > 1:
+            @pl.when(exists)
+            def _():
+                got(place, sr.at[(s - 1) * 2 + p])
+        if s < length:
+            after = a + sign
+            inside = jnp.logical_and(after >= 0, after < length)
+            to = jnp.clip(after, 0, length - 1) * 2 + b
+            at = s * 2 + p
+            guarded(jnp.logical_and(exists, inside), remote(
+                wb.at[p] if s == 1 else place, place, ss.at[at], sr.at[at], fs=to))
+
+    def send_weights(s):
+        for p in range(2):
+            for sign in (1, -1):
+                along(s, sign, p)
+                across(s, sign, p)
+
+    for p in range(2):
+        w_in[p].wait()
+        wb[p] = wf[p].astype(bf16)
 
     for k in range(n + 2):
         if 1 <= k < n:
@@ -129,8 +178,11 @@
             if group == 1:
                 product(0, me)
             for p in range(2):
-                w_in[p].wait()
-                wb[p] = wf[p].astype(bf16)
+                across(1, 1, p)
+        if k == n // 2:
+            for p in range(2):
+                for sign in (1, -1):
+                    along(1, sign, p)
         if k >= 3:
             j = origin(k - 2)
             got(rows(j, qc), c_r.at[k - 2])
@@ -141,42 +193,6 @@
         for k in range(n // group):
             product(k, k * group)
 
-    length = n // 2
-    a, b = me // 2, lax.rem(me, 2)
-    waits = []
-
-    def guarded(here, copy, start=True):
-        if start:
-            @pl.when(here)
-            def _():
-                copy.start()
-        waits.append((here, copy))
-
-    def block(chain, side):
-        safe = jnp.clip(chain, 0, length - 1)
-        return weights.at[safe * 2 + side]
-
-    def send_weights(s):
-        for sign, ss, sr in ((1, r_s, r_r), (-1, l_s, l_r)):
-            chain = a - sign * (s - 1)
-            exists = jnp.logical_and(chain >= 0, chain < length)
-            place = block(chain, b)
-            src = wb if s == 1 else place
-            slot = (s - 1) * 2 + (0 if sign == 1 else 1)
-            if s > 1:
-                @pl.when(exists)
-                def _():
-                    got(place, sr.at[s - 1])
-            if s < length:
-                after = a + sign
-                inside = jnp.logical_and(after >= 0, after < length)
-                to = jnp.clip(after, 0, length - 1) * 2 + b
-                guarded(jnp.logical_and(exists, inside), remote(src, place, ss.at[s], sr.at[s], fs=to))
-            if s > 1 or sign == 1:
-                guarded(exists, remote(src, place, y_s.at[slot], y_r.at[slot], fs=a * 2 + 1 - b))
-
-    send_weights(1)
-
     for p in range(2):
         c_in[p].wait()
 
@@ -205,8 +221,9 @@
         got(recvp.at[k], p_r.at[k])
         total = total + recvp[k].astype(f32)
     small_out[...] = total
-    first_new, second_new = moments(total, first[...], second[...])
-    dirs[0] = (first_new / (jnp.sqrt(second_new) + 1e-08)).astype(bf16)
+    for p, (first, second) in enumerate(((fi, si), (fg, sg))):
+        first_new, second_new = moments(total[p], first[...], second[...])
+        dirs[0, p] = (first_new / (jnp.sqrt(second_new) + 1e-08)).astype(bf16)
     for k in range(1, n):
         copy = remote(dirs.at[0], dirs.at[k], g_s.at[k], g_r.at[k], fs=peer(k))
         copy.start()
@@ -251,11 +268,12 @@
             if s == 1 and sign == -1:
                 continue
             chain = a - sign * (s - 1)
-            slot = (s - 1) * 2 + (0 if sign == 1 else 1)
-
-            @pl.when(jnp.logical_and(chain >= 0, chain < length))
-            def _():
-                got(block(chain, 1 - b), y_r.at[slot])
+            slot = ((s - 1) * 2 + (0 if sign == 1 else 1)) * 2
+            for p in range(2):
+
+                @pl.when(jnp.logical_and(chain >= 0, chain < length))
+                def _():
+                    got(block(chain, 1 - b, p), y_r.at[slot + p])
     for here, copy in waits:
         @pl.when(here)
         def _():
@@ -265,8 +283,8 @@
 
 
 def finish(
-    wi, wg, all_w, ball, dirs, small, squares, first, second, count_ref,
-    new_i, new_g, step_i, step_g, fi, si, fg, sg, copy_i, copy_g,
+    wi, wg, all_w, ball, dirs, small, squares, fi, si, fg, sg, count_ref,
+    new_i, new_g, step_i, step_g, fi_new, si_new, fg_new, sg_new, copy_i, copy_g,
 ):
     j = pl.program_id(0)
     me = lax.axis_index("fs")
@@ -274,9 +292,8 @@
 
     @pl.when(j == 0)
     def _():
-        first_new, second_new = moments(small[...], first[...], second[...])
-        fi[...], fg[...] = first_new[0], first_new[1]
-        si[...], sg[...] = second_new[0], second_new[1]
+        fi_new[...], si_new[...] = moments(small[0], fi[...], si[...])
+        fg_new[...], sg_new[...] = moments(small[1], fg[...], sg[...])
 
     for p, (w, new, step, copy) in enumerate(((wi, new_i, step_i, copy_i), (wg, new_g, step_g, copy_g))):
         mean = jnp.sum(squares[p], keepdims=True) * count_ref[0]
@@ -301,7 +318,6 @@
     wc, (rb, rank), rr = ci.shape[1], bi.shape, fi.shape[0]
     length = n // 2
     group = max(1, 128 // rb)
-    first, second = jnp.stack([fi, fg]), jnp.stack([si, sg])
     dma = pltpu.SemaphoreType.DMA
     all_w, ball, dirs, small, squares = pl.pallas_call(
         functools.partial(exchange, n, tp),
@@ -312,7 +328,7 @@
             jax.ShapeDtypeStruct((2, rr, wc), f32),
             jax.ShapeDtypeStruct((2, 8, 128), f32),
         ),
-        in_specs=[ANY] * 7 + [VMEM] * 2,
+        in_specs=[ANY] * 7 + [VMEM] * 4,
         out_specs=(ANY, ANY, VMEM, VMEM, VMEM),
         scratch_shapes=[
             pltpu.VMEM((n // group, tokens, rb * group), bf16),
@@ -331,13 +347,13 @@
         ]
         + [dma((n,))] * 12
         + [dma((tp,))] * 2
-        + [dma((length + 1,))] * 4
-        + [dma((2 * length,))] * 2,
+        + [dma((2 * length,))] * 4
+        + [dma((4 * length,))] * 2,
         compiler_params=pltpu.CompilerParams(
             collective_id=0, has_side_effects=True, vmem_limit_bytes=56 * 1024 * 1024
         ),
         name="exchange",
-    )(x, ci, cg, wi, wg, bi, bg, first, second)
+    )(x, ci, cg, wi, wg, bi, bg, fi, si, fg, sg)
 
     def whole(*shape):
         return pl.BlockSpec(shape, lambda j: (0,) * len(shape))
@@ -353,15 +369,15 @@
             whole(rb, wc), whole(rb, wc),
             pl.BlockSpec((1, 2, rb, wc), lambda j: (j, 0, 0, 0)),
             pl.BlockSpec((1, rb, 2 * rank), lambda j: (j, 0, 0)),
-            whole(2, rank, wc), whole(2, rr, wc), whole(2, 8, 128), whole(2, rr, wc), whole(2, rr, wc),
+            whole(2, rank, wc), whole(2, rr, wc), whole(2, 8, 128), *[whole(rr, wc)] * 4,
             pl.BlockSpec(memory_space=pltpu.SMEM),
         ],
         out_specs=tuple(whole(rb, wc) for _ in range(4))
         + tuple(whole(rr, wc) for _ in range(4))
         + tuple(pl.BlockSpec((rb, wc), lambda j: (j, 0)) for _ in range(2)),
-        compiler_params=pltpu.CompilerParams(vmem_limit_bytes=40 * 1024 * 1024),
+        compiler_params=pltpu.CompilerParams(vmem_limit_bytes=63 * 1024 * 1024),
         name="finish",
-    )(wi, wg, all_w, ball, dirs, small, squares, first, second, count)
+    )(wi, wg, all_w, ball, dirs, small, squares, fi, si, fg, sg, count)
 
 
 def solution(mesh):

time: 123 us -> 101 us (0.82)
  Pallas kernels: 114 us -> 100 us
  local copies, waits for them, and re-layouts: 6.43 us -> 0 us
  other arithmetic: 1.65 us -> 0 us
    pallas_call x1, Pallas kernels: 107 us -> 89.7 us  [shards(): pl.pallas_call(functools.partial(exchange, n, tp), out_shape=(jax.ShapeDt...]
    unnamed x18 -> x0, local copies, waits for them, and re-layouts: 6.43 us -> none
    pallas_call x1, Pallas kernels: 7.03 us -> 10.6 us  [shards(): pl.pallas_call(finish, grid=(n,), out_shape=tuple((jax.ShapeDtypeStruct((...]
    another operation x1 -> x0, other arithmetic: 1.65 us -> none  [shards(): first, second = (jnp.stack([fi, fg]), jnp.stack([si, sg]))]
where the time goes in v2:
time: 101 us
  Pallas kernels  100 us (99%)
    pallas_call x1, Pallas kernels, shards(): pl.pallas_call(functools.partial(exchange, n, tp), out_shape=(jax.ShapeDt...  89.7 us
    pallas_call x1, Pallas kernels, shards(): pl.pallas_call(finish, grid=(n,), out_shape=tuple((jax.ShapeDtypeStruct((...  10.6 us

profile of v2, /device:TPU:0, one launch (start us, length us, event | category | flops | bytes accessed | tf_op | source)
XLA Modules:
  0.0 101.0 jit_solution(5332173903729522897)
XLA Ops:
  0.6 89.7 %exchange.1 = (bf16[8,2,256,512]{3,2,1,0:T(8,128)(2,1)}, bf16[8,256,512]{2,1,0:T(8,128)(2,1)}, bf16[2,256,512]{2,1,0:T(8,128)(2,1)}, f32[2,32,512]{2,1,0:T(8,128)}, f32[2,8,128]{2,1,0:T(8,128)}) custom-call(bf16[2048,2048]{1,0:T(8,128)(2,1)} %x_hbm.1, bf16[2048,512]{1,0:T(8,128)(2,1)} %ci_hbm.1, bf16[2048,512]{1,0:T(8,128)(2,1)} %cg_hbm.1, f32[256,512]{1,0:T(8,128)} %wi.1, ...), custom_call_target="tpu_custom_call" | custom-call | tf_op jit(solution)/shard_map/exchange/pallas_call | solution.py:322
  90.3 10.6 %finish.1 = (f32[256,512]{1,0:T(8,128)}, f32[256,512]{1,0:T(8,128)}, f32[256,512]{1,0:T(8,128)}, f32[256,512]{1,0:T(8,128)}, f32[32,512]{1,0:T(8,128)}, /*index=...) custom-call(f32[256,512]{1,0:T(8,128)} %wi.1, ...), custom_call_target="tpu_custom_call" | custom-call | tf_op jit(solution)/shard_map/finish/pallas_call | solution.py:362

commit v3 on v2

--- a/solution.py
+++ b/solution.py
@@ -179,7 +179,7 @@
                 product(0, me)
             for p in range(2):
                 across(1, 1, p)
-        if k == n // 2:
+        if k == 1:
             for p in range(2):
                 for sign in (1, -1):
                     along(1, sign, p)
@@ -193,6 +193,8 @@
         for k in range(n // group):
             product(k, k * group)
 
+    send_weights(2)
+
     for p in range(2):
         c_in[p].wait()
 
@@ -214,7 +216,6 @@
         copy.start()
         pending.append(copy)
     out_basis = local(ball, basis_out, osem.at[0])
-    send_weights(2)
     own = pl.ds(pl.multiple_of(me * rr, rr), rr)
     total = acc[:, own, :]
     for k in range(1, n):

time: 101 us -> 104 us (1.030)
  Pallas kernels: 100 us -> 103 us
    pallas_call x1, Pallas kernels: 89.7 us -> 92.8 us  [shards(): pl.pallas_call(functools.partial(exchange, n, tp), out_shape=(jax.ShapeDt...]
where the time goes in v3:
time: 104 us
  Pallas kernels  103 us (99%)
    pallas_call x1, Pallas kernels, shards(): pl.pallas_call(functools.partial(exchange, n, tp), out_shape=(jax.ShapeDt...  92.8 us
    pallas_call x1, Pallas kernels, shards(): pl.pallas_call(finish, grid=(n,), out_shape=tuple((jax.ShapeDtypeStruct((...  10.6 us

profile of v3, /device:TPU:0, one launch (start us, length us, event | category | flops | bytes accessed | tf_op | source)
XLA Modules:
  0.0 104.1 jit_solution(7982572908845675917)
XLA Ops:
  0.6 92.8 %exchange.1 = (bf16[8,2,256,512]{3,2,1,0:T(8,128)(2,1)}, bf16[8,256,512]{2,1,0:T(8,128)(2,1)}, bf16[2,256,512]{2,1,0:T(8,128)(2,1)}, f32[2,32,512]{2,1,0:T(8,128)}, f32[2,8,128]{2,1,0:T(8,128)}) custom-call(bf16[2048,2048]{1,0:T(8,128)(2,1)} %x_hbm.1, bf16[2048,512]{1,0:T(8,128)(2,1)} %ci_hbm.1, bf16[2048,512]{1,0:T(8,128)(2,1)} %cg_hbm.1, f32[256,512]{1,0:T(8,128)} %wi.1, ...), custom_call_target="tpu_custom_call" | custom-call | tf_op jit(solution)/shard_map/exchange/pallas_call | solution.py:323
  93.5 10.6 %finish.1 = (f32[256,512]{1,0:T(8,128)}, f32[256,512]{1,0:T(8,128)}, f32[256,512]{1,0:T(8,128)}, f32[256,512]{1,0:T(8,128)}, f32[32,512]{1,0:T(8,128)}, /*index=...) custom-call(f32[256,512]{1,0:T(8,128)} %wi.1, ...), custom_call_target="tpu_custom_call" | custom-call | tf_op jit(solution)/shard_map/finish/pallas_call | solution.py:363
